TPU v7x, 32 devices: a whole 2x2x4 slice. The times are simulated.
32 devices in a mesh: fs: 8 (over z, y), tp: 4 (over x, core).
Axes of the slice: x: 2, y: 2, z: 4, core: 2. Of those that a mesh axis runs over, the one named last changes fastest.
Arguments:
- tokens: bfloat16 [8192, 2048], P('fs', 'tp'), may hold values from -6 to 6
- mix_gain: float32 [2048], replicated, may hold values from 0.1 to 1.9
- in_weight: float32 [2048, 1024], P('fs', 'tp'), may hold values from -0.125 to 0.125
- in_scale: float32 [1024], P('tp'), may hold values from 0.4 to 2.5
- out_weight: float32 [1024, 2048], P('tp', 'fs'), may hold values from -0.1875 to 0.1875
- out_scale: float32 [2048], P('fs'), may hold values from 0.4 to 2.5
- ffn_gain: float32 [2048], replicated, may hold values from 0.1 to 1.9
- gate_weight: float32 [2048, 6144], P('fs', 'tp'), may hold values from -0.125 to 0.125
- gate_scale: float32 [6144], P('tp'), may hold values from 0.4 to 2.5
- up_weight: float32 [2048, 6144], P('fs', 'tp'), may hold values from -0.125 to 0.125
- up_scale: float32 [6144], P('tp'), may hold values from 0.4 to 2.5
- down_weight: float32 [6144, 2048], P('tp', 'fs'), may hold values from -0.078125 to 0.078125
- down_scale: float32 [2048], P('fs'), may hold values from 0.4 to 2.5
Outputs:
- layer_out: bfloat16 [8192, 2048], P('fs', 'tp')
All inputs are finite; a program needn't handle non-finite values.
Results may differ from a plain program's by a relative error of at most 0.023.
Values may be sent and summed in bfloat16 or wider, within the bound.
A program may use at most 128 MiB of HBM per device.

v0:
```python
import jax
import jax.numpy as jnp
from jax import lax
from jax.sharding import PartitionSpec as P

D = 2048
GROUPS = 4
GRID_W = 64
GC = 256
WINDOWS = (2, 4, 8, 16)
EPSILON = 1e-06


def box_matrix(length, window):
    position = jnp.arange(length, dtype=jnp.int32)
    lower_end = jnp.clip(position - window // 2, 0, length)
    upper_end = jnp.clip(position + (window - window // 2), 0, length)
    inside = (position[None, :] >= lower_end[:, None]) & (position[None, :] < upper_end[:, None])
    return inside.astype(jnp.float32) / (upper_end - lower_end).astype(jnp.float32)[:, None]


def pooled_differences(channels, channel_offset):
    tokens_here, extent = channels.shape
    lattice = channels.reshape(tokens_here // GRID_W, GRID_W, extent)
    group_of = (channel_offset + jnp.arange(extent, dtype=jnp.int32)) // GC
    result = jnp.zeros_like(lattice)
    for group in range(GROUPS):
        window = WINDOWS[group]
        across = jnp.einsum(
            "jk,akc->ajc", box_matrix(GRID_W, window), lattice, precision=lax.Precision.HIGHEST
        )
        smoothed = jnp.einsum(
            "ab,bjc->ajc",
            box_matrix(lattice.shape[0], window),
            across,
            precision=lax.Precision.HIGHEST,
        )
        result = jnp.where((group_of == group)[None, None, :], smoothed, result)
    return (result - lattice).reshape(tokens_here, extent).astype(jnp.bfloat16)


def fold_rows(features, gain, weights):
    widened = lax.all_gather(features, "tp", axis=1, tiled=True).astype(jnp.float32)
    squares = jnp.sum(widened * widened, axis=1)
    scaled = (widened * gain).astype(jnp.bfloat16)
    totals = tuple(
        (jnp.dot(scaled, weight, preferred_element_type=jnp.float32) for weight in weights)
    )
    totals, squares = (totals, squares)
    inverse_rms = lax.rsqrt(squares / D + EPSILON)[:, None]
    return tuple((total * inverse_rms for total in totals))


def column_product(hidden, weight_columns, scales):
    partial_value = (
        jnp.dot(
            hidden,
            lax.all_gather(weight_columns, "fs", axis=1, tiled=True),
            preferred_element_type=jnp.float32,
        )
        * scales
    )
    return lax.psum_scatter(
        partial_value.astype(jnp.bfloat16), "tp", scatter_dimension=1, tiled=True
    ).astype(jnp.float32)


def local(
    tokens,
    mix_gain,
    in_weight,
    in_scale,
    out_weight,
    out_scale,
    ffn_gain,
    gate_weight,
    gate_scale,
    up_weight,
    up_scale,
    down_weight,
    down_scale,
):
    out_scales, down_scales = (
        lax.all_gather(out_scale, "fs", axis=0, tiled=True),
        lax.all_gather(down_scale, "fs", axis=0, tiled=True),
    )
    in_full, gate_full, up_full = (
        lax.all_gather(in_weight.astype(jnp.bfloat16), "fs", axis=0, tiled=True),
        lax.all_gather(gate_weight.astype(jnp.bfloat16), "fs", axis=0, tiled=True),
        lax.all_gather(up_weight.astype(jnp.bfloat16), "fs", axis=0, tiled=True),
    )
    (channels,) = fold_rows(tokens, mix_gain, (in_full,))
    channels = channels * in_scale
    pooled = pooled_differences(channels, lax.axis_index("tp") * channels.shape[1])
    mixed = column_product(pooled, out_weight.astype(jnp.bfloat16), out_scales)
    residual = (tokens.astype(jnp.float32) + mixed).astype(jnp.bfloat16)
    gate_value, up_value = fold_rows(residual, ffn_gain, (gate_full, up_full))
    gate_value = gate_value * gate_scale
    up_value = up_value * up_scale
    hidden = (jax.nn.silu(gate_value) * up_value).astype(jnp.bfloat16)
    channel_out = column_product(hidden, down_weight.astype(jnp.bfloat16), down_scales)
    return (residual.astype(jnp.float32) + channel_out).astype(jnp.bfloat16)


def solution(mesh):
    return jax.shard_map(
        local,
        mesh=mesh,
        in_specs=(
            P("fs", "tp"),
            P(),
            P("fs", "tp"),
            P("tp"),
            P("tp", "fs"),
            P("fs"),
            P(),
            P("fs", "tp"),
            P("tp"),
            P("fs", "tp"),
            P("tp"),
            P("tp", "fs"),
            P("fs"),
        ),
        out_specs=P("fs", "tp"),
        check_vma=False,
    )
```

profile of v0, /device:TPU:0, one launch (start us, length us, event | category | flops | bytes accessed | tf_op | source)
XLA Modules:
  0.0 587.0 jit_solution(10302616835622095069)
XLA Ops:
  6.5 0.7 all-gather.10.cloned.1.call-update
  7.3 0.0 all-gather.12.cloned.1.call-start
  7.3 1.6 convert_element_type.145
  8.9 0.0 all-gather.12.cloned.1.call-update
  9.0 0.0 all-gather.14.cloned.1.call-start
  9.0 1.6 convert_element_type.162
  10.6 0.0 reduce-scatter.3.cloned.1.call-start
  11.0 22.6 %all-gather = f32[8,1,256]{2,1,0:T(1,128)S(1)} all-gather(f32[1,1,256]{2,1,0:T(1,128)} %bitcast.61), channel_id=1, replica_groups=mesh['fs'=8,'tp'=4] {'fs'}, dimensions={0}, use_global_device_ids=true | all-gather | bytes 9216 | tf_op jit(solution)/shard_map/all_gather | solution.py:84
  33.5 12.6 %all-gather.10.cloned.1.call-done = bf16[1024,2048]{1,0:T(8,128)(2,1)} async-done(((bf16[1024,512]{1,0:T(8,128)(2,1)}), bf16[1024,2048]{1,0:T(8,128)(2,1)}) %all-gather.10.cloned.1.call-update) | async-done | bytes 4194320 | tf_op jit(solution)/shard_map/all_gather | solution.py:43
  46.1 3.1 fusion.1
  49.2 39.4 %all-gather.12.cloned.1.call-done = bf16[2048,256]{1,0:T(8,128)(2,1)} async-done(((bf16[256,256]{1,0:T(8,128)(2,1)}), bf16[2048,256]{1,0:T(8,128)(2,1)}) %all-gather.12.cloned.1.call-update) | async-done | bytes 1048592 | tf_op jit(solution)/shard_map/all_gather | solution.py:88
  88.5 3.7 fusion.14
  92.3 1.1 convolution_bitcast_fusion
  93.4 1.1 convolution_bitcast_fusion.1
  94.4 1.1 convolution_bitcast_fusion.2
  95.5 1.1 convolution_bitcast_fusion.3
  96.6 1.5 convolution_select_fusion
  98.1 1.5 convolution_select_fusion.1
  99.6 1.5 convolution_select_fusion.2
  101.1 2.3 fusion.17
  103.4 0.2 copy.22
  103.5 25.2 %all-gather.14.cloned.1.call-done = bf16[256,2048]{1,0:T(8,128)(2,1)} async-done(((bf16[256,256]{1,0:T(8,128)(2,1)}), bf16[256,2048]{1,0:T(8,128)(2,1)}) %all-gather.14.cloned.1.call-update) | async-done | bytes 1048592 | tf_op jit(solution)/shard_map/all_gather | solution.py:58
  128.7 4.5 multiply_convert_fusion.1
  133.3 0.0 reduce-scatter.3.cloned.1.call-update
  133.3 0.0 all-gather.16.cloned.1.call-start
  133.4 43.5 %reduce-scatter.3.cloned.1.call-done = bf16[1024,512]{1,0:T(8,128)(2,1)} async-done(((bf16[1024,2048]{1,0:T(8,128)(2,1)}), bf16[1024,512]{1,0:T(8,128)(2,1)}) %reduce-scatter.3.cloned.1.call-update) | async-done | bytes 1048592 | tf_op jit(solution)/shard_map/reduce_scatter | solution.py:63
  176.9 2.5 add_convert_fusion.1
  179.4 0.0 all-gather.16.cloned.1.call-update
  179.4 0.0 all-gather.18.cloned.1.call-start
  179.5 1.0 convert_element_type.169
  180.5 0.0 all-gather.18.cloned.1.call-update
  180.5 0.0 all-gather.20.cloned.1.call-start
  180.5 2.4 convert_element_type.170
  182.9 0.0 all-gather.20.cloned.1.call-update
  183.0 0.0 all-gather.22.cloned.1.call-start
  183.0 1.0 convert_element_type.172
  184.0 0.0 all-gather.22.cloned.1.call-update
  184.0 0.0 reduce-scatter.5.cloned.1.call-start
  184.1 20.5 %all-gather.1 = f32[8,1,256]{2,1,0:T(1,128)S(1)} all-gather(f32[1,1,256]{2,1,0:T(1,128)S(1)} %bitcast.62), channel_id=1, replica_groups=mesh['fs'=8,'tp'=4] {'fs'}, dimensions={0}, use_global_device_ids=true | all-gather | bytes 9216 | tf_op jit(solution)/shard_map/all_gather | solution.py:85
  204.6 9.4 %all-gather.16.cloned.1.call-done = bf16[1024,2048]{1,0:T(8,128)(2,1)} async-done(((bf16[1024,512]{1,0:T(8,128)(2,1)}), bf16[1024,2048]{1,0:T(8,128)(2,1)}) %all-gather.16.cloned.1.call-update) | async-done | bytes 4194320 | tf_op jit(solution)/shard_map/all_gather | solution.py:43
  214.0 3.1 fusion.3
  217.1 97.7 %all-gather.18.cloned.1.call-done = bf16[2048,1536]{1,0:T(8,128)(2,1)} async-done(((bf16[256,1536]{1,0:T(8,128)(2,1)}), bf16[2048,1536]{1,0:T(8,128)(2,1)}) %all-gather.18.cloned.1.call-update) | async-done | bytes 6291472 | tf_op jit(solution)/shard_map/all_gather | solution.py:89
  314.8 11.7 %fusion.8 = f32[1024,1536]{1,0:T(8,128)} fusion(bf16[2048,1536]{1,0:T(8,128)(2,1)} %all-gather.18.cloned.1.call-done, bf16[1024,2048]{1,0:T(8,128)(2,1)} %all-gather.16.cloned.1.call-done, f32[2048]{0:T(1024)S(1)} %copy-done.6), kind=kOutput, calls=%fused_computation.13 | convolution fusion | flops 6448742400 | bytes 16785408 | tf_op jit(solution)/shard_map/dot_general | solution.py:47
  326.5 87.4 %all-gather.20.cloned.1.call-done = bf16[2048,1536]{1,0:T(8,128)(2,1)} async-done(((bf16[256,1536]{1,0:T(8,128)(2,1)}), bf16[2048,1536]{1,0:T(8,128)(2,1)}) %all-gather.20.cloned.1.call-update) | async-done | bytes 6291472 | tf_op jit(solution)/shard_map/all_gather | solution.py:90
  413.8 99.7 %all-gather.22.cloned.1.call-done = bf16[1536,2048]{1,0:T(8,128)(2,1)} async-done(((bf16[1536,256]{1,0:T(8,128)(2,1)}), bf16[1536,2048]{1,0:T(8,128)(2,1)}) %all-gather.22.cloned.1.call-update) | async-done | bytes 6291472 | tf_op jit(solution)/shard_map/all_gather | solution.py:58
  513.6 21.6 %multiply_convert_fusion = bf16[1024,2048]{1,0:T(8,128)(2,1)} fusion(bf16[1536,2048]{1,0:T(8,128)(2,1)} %all-gather.22.cloned.1.call-done, f32[2048]{0:T(1024)S(1)} %bitcast.60, f32[1024,1536]{1,0:T(8,128)} %fusion.8, bf16[2048,1536]{1,0:T(8,128)(2,1)} %all-gather.20.cloned.1.call-done, bf16[1024,2048]{1,0:T(8,128)(2,1)} %all-gather.16.cloned.1.call-done, ...), kind=kOutput, calls=%fused_computation.8 | convolution fusion | flops 12911116288 | bytes 27295744 | tf_op jit(solution)/shard_map/dot_general | solution.py:56
  535.2 42.8 %reduce-scatter.5.cloned.1.call-done = bf16[1024,512]{1,0:T(8,128)(2,1)} async-done(((bf16[1024,2048]{1,0:T(8,128)(2,1)}), bf16[1024,512]{1,0:T(8,128)(2,1)}) %reduce-scatter.5.cloned.1.call-update) | async-done | bytes 1048592 | tf_op jit(solution)/shard_map/reduce_scatter | solution.py:63
  578.0 2.5 add_convert_fusion
  (43 shorter events, 0.2 us)
Async XLA Ops:
  6.5 82.0 %copy-start.5 = (f32[2048]{0:T(1024)S(1)}, f32[2048]{0:T(1024)}, u32[]{:S(2)}) copy-start(f32[2048]{0:T(1024)} %param.14) | copy-start | bytes 24580
  6.5 82.0 %copy-start.9 = (f32[256]{0:T(256)S(1)}, f32[256]{0:T(256)}, u32[]{:S(2)}) copy-start(f32[256]{0:T(256)} %param.16) | copy-start | bytes 3076
  6.5 39.6 %all-gather.10.cloned.1.call-start = ((), (), s32[]{:S(2)}) async-start(), calls=%async_computation.2 | async-start | bytes 5242880 | tf_op jit(solution)/shard_map/all_gather | solution.py:43
  7.3 81.3 %all-gather.12.cloned.1.call-start = ((), (), s32[]{:S(2)}) async-start(), calls=%async_computation.3 | async-start | bytes 1179648 | tf_op jit(solution)/shard_map/all_gather | solution.py:88
  9.0 119.8 %all-gather.14.cloned.1.call-start = ((), (), s32[]{:S(2)}) async-start(), calls=%async_computation.4 | async-start | bytes 1179648 | tf_op jit(solution)/shard_map/all_gather | solution.py:58
  10.6 166.2 %reduce-scatter.3.cloned.1.call-start = ((), (), s32[]{:S(2)}) async-start(), calls=%async_computation.5 | async-start | bytes 5242880 | tf_op jit(solution)/shard_map/reduce_scatter | solution.py:63
  128.7 48.1 %copy-start.1 = (bf16[1024,512]{1,0:T(8,128)(2,1)S(1)}, bf16[1024,512]{1,0:T(8,128)(2,1)}, u32[]{:S(2)}) copy-start(bf16[1024,512]{1,0:T(8,128)(2,1)} %param.13) | copy-start | bytes 3145732
  133.3 46.2 %copy-start.2 = (f32[256,1536]{1,0:T(8,128)S(1)}, f32[256,1536]{1,0:T(8,128)}, u32[]{:S(2)}) copy-start(f32[256,1536]{1,0:T(8,128)} %param.20) | copy-start | bytes 4718596
  133.3 50.8 %copy-start.4 = (f32[256]{0:T(256)S(1)}, f32[256]{0:T(256)}, u32[]{:S(2)}) copy-start(f32[256]{0:T(256)} %param.25) | copy-start | bytes 3076
  133.3 80.7 %all-gather.16.cloned.1.call-start = ((), (), s32[]{:S(2)}) async-start(), calls=%async_computation.6 | async-start | bytes 5242880 | tf_op jit(solution)/shard_map/all_gather | solution.py:43
  179.4 3.6 copy-start.3
  179.4 135.4 %copy-start.6 = (f32[2048]{0:T(1024)S(1)}, f32[2048]{0:T(1024)}, u32[]{:S(2)}) copy-start(f32[2048]{0:T(1024)} %param.19) | copy-start | bytes 24580
  179.4 135.4 %all-gather.18.cloned.1.call-start = ((), (), s32[]{:S(2)}) async-start(), calls=%async_computation.7 | async-start | bytes 7077888 | tf_op jit(solution)/shard_map/all_gather | solution.py:89
  180.5 233.4 %all-gather.20.cloned.1.call-start = ((), (), s32[]{:S(2)}) async-start(), calls=%async_computation.8 | async-start | bytes 7077888 | tf_op jit(solution)/shard_map/all_gather | solution.py:90
  183.0 330.6 %all-gather.22.cloned.1.call-start = ((), (), s32[]{:S(2)}) async-start(), calls=%async_computation.9 | async-start | bytes 7077888 | tf_op jit(solution)/shard_map/all_gather | solution.py:58
  184.0 394.0 %reduce-scatter.5.cloned.1.call-start = ((), (), s32[]{:S(2)}) async-start(), calls=%async_computation.10 | async-start | bytes 5242880 | tf_op jit(solution)/shard_map/reduce_scatter | solution.py:63
  217.1 296.5 %copy-start.7 = (f32[1536]{0:T(1024)S(1)}, f32[1536]{0:T(1024)}, u32[]{:S(2)}) copy-start(f32[1536]{0:T(1024)} %param.23) | copy-start | bytes 18436
  217.1 296.5 %copy-start.8 = (f32[1536]{0:T(1024)S(1)}, f32[1536]{0:T(1024)}, u32[]{:S(2)}) copy-start(f32[1536]{0:T(1024)} %param.21) | copy-start | bytes 18436
  513.6 64.4 %copy-start = (bf16[1024,512]{1,0:T(8,128)(2,1)S(1)}, bf16[1024,512]{1,0:T(8,128)(2,1)}, u32[]{:S(2)}) copy-start(bf16[1024,512]{1,0:T(8,128)(2,1)} %add_convert_fusion.1) | copy-start | bytes 3145732
Sparse Core Ops, SparseCore 0:
  8.9 37.1 all-gather.9
  48.2 40.2 all-gather.11
  90.6 38.0 all-gather.13
  133.4 43.4 reduce-scatter.2
  179.5 34.4 all-gather.15
  216.0 98.6 all-gather.17
  316.9 96.8 all-gather.19
  415.9 97.6 all-gather.21
  535.3 42.5 reduce-scatter.4
where the time goes:
time: 587 us
  waiting for transfers between devices  458 us (78%)
  matrix products  52.6 us (9%)
  blocking collectives  43.1 us (7%)
  other arithmetic  18.9 us (3%)
  between operations  13.5 us (2%)
    all_gather x2, waiting for transfers between devices, column_product(): lax.all_gather(weight_columns, 'fs', axis=1, tiled=True)  125 us
    all_gather x1, waiting for transfers between devices, local(): lax.all_gather(gate_weight.astype(jnp.bfloat16), 'fs', axis=0, tiled=True)  97.7 us
    all_gather x1, waiting for transfers between devices, local(): lax.all_gather(up_weight.astype(jnp.bfloat16), 'fs', axis=0, tiled=True)  87.4 us
    reduce_scatter x2, waiting for transfers between devices, column_product(): lax.psum_scatter(partial_value.astype(jnp.bfloat16), 'tp', scatter_dimens...  86.3 us
    all_gather x1, waiting for transfers between devices, local(): lax.all_gather(in_weight.astype(jnp.bfloat16), 'fs', axis=0, tiled=True)  39.4 us
    dot_general x2, matrix products, column_product(): jnp.dot(hidden, lax.all_gather(weight_columns, 'fs', axis=1, tiled=True),...  26.1 us
    all_gather x1, blocking collectives, local(): lax.all_gather(out_scale, 'fs', axis=0, tiled=True)  22.6 us
    all_gather x2, waiting for transfers between devices, fold_rows(): lax.all_gather(features, 'tp', axis=1, tiled=True).astype(jnp.float32)  22 us
  transfers between devices with their start and end apart: 9, of which 9 were waited for; matrix products, arithmetic and copies ran while one was open for 7% of the time, Pallas kernels for 0%

commit v1 on v0

--- a/solution.py
+++ b/solution.py
@@ -9,6 +9,18 @@
 GC = 256
 WINDOWS = (2, 4, 8, 16)
 EPSILON = 1e-06
+
+
+def collect(x, axis, dim):
+    ways, here = (lax.axis_size(axis), lax.axis_index(axis))
+    grown, reach = (x, 1)
+    while reach < ways:
+        theirs = lax.ppermute(grown, axis, [(d, d ^ reach) for d in range(ways)])
+        mine_first = jnp.concatenate([grown, theirs], axis=dim)
+        theirs_first = jnp.concatenate([theirs, grown], axis=dim)
+        grown = jnp.where(here & reach == 0, mine_first, theirs_first)
+        reach = 2 * reach
+    return grown
 
 
 def box_matrix(length, window):
@@ -85,7 +97,7 @@
         lax.all_gather(down_scale, "fs", axis=0, tiled=True),
     )
     in_full, gate_full, up_full = (
-        lax.all_gather(in_weight.astype(jnp.bfloat16), "fs", axis=0, tiled=True),
+        collect(in_weight.astype(jnp.bfloat16), "fs", 0),
         lax.all_gather(gate_weight.astype(jnp.bfloat16), "fs", axis=0, tiled=True),
         lax.all_gather(up_weight.astype(jnp.bfloat16), "fs", axis=0, tiled=True),
     )

time: 587 us -> 546 us (0.930)
  waiting for transfers between devices: 458 us -> 415 us
    all_gather x1 -> x0, waiting for transfers between devices: 39.4 us -> none  [local(): lax.all_gather(in_weight.astype(jnp.bfloat16), 'fs', axis=0, tiled=True)]
    ppermute x0 -> x3, waiting for transfers between devices: none -> 9.03 us  [collect(): theirs = lax.ppermute(grown, axis, [(d, d ^ reach) for d in range(ways)])]
    all_gather x2, waiting for transfers between devices: 125 us -> 116 us  [column_product(): lax.all_gather(weight_columns, 'fs', axis=1, tiled=True)]
  transfers between devices with their start and end apart: 9 -> 11, of which waited for: 9 -> 10; matrix products, arithmetic and copies ran while one was open for 7% -> 7% of each run, Pallas kernels for 0% -> 0%
where the time goes in v1:
time: 546 us
  waiting for transfers between devices  415 us (76%)
  matrix products  52.3 us (10%)
  blocking collectives  40.5 us (7%)
  other arithmetic  18.6 us (3%)
  between operations  13.8 us (3%)
    all_gather x2, waiting for transfers between devices, column_product(): lax.all_gather(weight_columns, 'fs', axis=1, tiled=True)  116 us
    all_gather x1, waiting for transfers between devices, local(): lax.all_gather(gate_weight.astype(jnp.bfloat16), 'fs', axis=0, tiled=True)  97.7 us
    all_gather x1, waiting for transfers between devices, local(): lax.all_gather(up_weight.astype(jnp.bfloat16), 'fs', axis=0, tiled=True)  87.2 us
    reduce_scatter x2, waiting for transfers between devices, column_product(): lax.psum_scatter(partial_value.astype(jnp.bfloat16), 'tp', scatter_dimens...  86.3 us
    dot_general x2, matrix products, column_product(): jnp.dot(hidden, lax.all_gather(weight_columns, 'fs', axis=1, tiled=True),...  26.1 us
    all_gather x1, blocking collectives, local(): lax.all_gather(down_scale, 'fs', axis=0, tiled=True)  20.5 us
    all_gather x1, blocking collectives, local(): lax.all_gather(out_scale, 'fs', axis=0, tiled=True)  20.1 us
    all_gather x2, waiting for transfers between devices, fold_rows(): lax.all_gather(features, 'tp', axis=1, tiled=True).astype(jnp.float32)  18.3 us
  transfers between devices with their start and end apart: 11, of which 10 were waited for; matrix products, arithmetic and copies ran while one was open for 7% of the time, Pallas kernels for 0%

profile of v1, /device:TPU:0, one launch (start us, length us, event | category | flops | bytes accessed | tf_op | source)
XLA Modules:
  0.0 546.0 jit_solution(5732679175274013854)
XLA Ops:
  6.5 0.7 all-gather.9.cloned.1.call-update
  7.3 0.0 all-gather.11.cloned.1.call-start
  7.3 1.0 convert_element_type.145
  8.3 3.1 collective-permute-start
  11.3 1.6 convert_element_type.162
  13.0 0.0 all-gather.11.cloned.1.call-update
  13.0 0.0 reduce-scatter.3.cloned.1.call-start
  13.3 1.6 collective-permute-done
  14.8 0.1 maximum_select_fusion.3
  14.9 1.9 collective-permute-start.1
  16.8 20.1 %all-gather = f32[8,1,256]{2,1,0:T(1,128)S(1)} all-gather(f32[1,1,256]{2,1,0:T(1,128)} %bitcast.60), channel_id=1, replica_groups=mesh['fs'=8,'tp'=4] {'fs'}, dimensions={0}, use_global_device_ids=true | all-gather | bytes 9216 | tf_op jit(solution)/shard_map/all_gather | solution.py:96
  36.9 0.2 maximum_select_fusion.2
  37.1 0.1 collective-permute-start.2
  37.2 8.9 %all-gather.9.cloned.1.call-done = bf16[1024,2048]{1,0:T(8,128)(2,1)} async-done(((bf16[1024,512]{1,0:T(8,128)(2,1)}), bf16[1024,2048]{1,0:T(8,128)(2,1)}) %all-gather.9.cloned.1.call-update) | async-done | bytes 4194320 | tf_op jit(solution)/shard_map/all_gather | solution.py:55
  46.1 3.1 fusion.1
  49.2 7.5 %collective-permute-done.2 = bf16[1024,256]{1,0:T(8,128)(2,1)S(1)} collective-permute-done((bf16[1024,256]{1,0:T(8,128)(2,1)S(1)}, bf16[1024,256]{1,0:T(8,128)(2,1)S(1)}, u32[]{:S(2)}, u32[]{:S(2)}) %collective-permute-start.2) | collective-permute-done | bytes 524320 | tf_op jit(solution)/shard_map/ppermute | solution.py:18
  56.7 3.5 fusion.14
  60.1 1.1 convolution_bitcast_fusion
  61.2 1.0 convolution_bitcast_fusion.1
  62.3 1.1 convolution_bitcast_fusion.2
  63.3 1.1 convolution_bitcast_fusion.3
  64.4 1.5 convolution_select_fusion
  65.9 1.5 convolution_select_fusion.1
  67.4 1.5 convolution_select_fusion.2
  68.9 2.3 fusion.17
  71.2 0.2 copy.22
  71.3 16.2 %all-gather.11.cloned.1.call-done = bf16[256,2048]{1,0:T(8,128)(2,1)} async-done(((bf16[256,256]{1,0:T(8,128)(2,1)}), bf16[256,2048]{1,0:T(8,128)(2,1)}) %all-gather.11.cloned.1.call-update) | async-done | bytes 1048592 | tf_op jit(solution)/shard_map/all_gather | solution.py:70
  87.6 4.5 multiply_convert_fusion.1
  92.2 0.0 all-gather.13.cloned.1.call-start
  92.2 43.5 %reduce-scatter.3.cloned.1.call-done = bf16[1024,512]{1,0:T(8,128)(2,1)} async-done(((bf16[1024,2048]{1,0:T(8,128)(2,1)}), bf16[1024,512]{1,0:T(8,128)(2,1)}) %reduce-scatter.3.cloned.1.call-update) | async-done | bytes 1048592 | tf_op jit(solution)/shard_map/reduce_scatter | solution.py:75
  135.7 2.5 add_convert_fusion.1
  138.2 0.0 all-gather.15.cloned.1.call-start
  138.3 1.0 convert_element_type.169
  139.3 0.0 all-gather.17.cloned.1.call-start
  139.4 2.4 convert_element_type.170
  141.8 0.0 all-gather.19.cloned.1.call-start
  141.9 1.0 convert_element_type.172
  142.9 0.0 reduce-scatter.5.cloned.1.call-start
  142.9 20.5 %all-gather.1 = f32[8,1,256]{2,1,0:T(1,128)S(1)} all-gather(f32[1,1,256]{2,1,0:T(1,128)S(1)} %bitcast.61), channel_id=1, replica_groups=mesh['fs'=8,'tp'=4] {'fs'}, dimensions={0}, use_global_device_ids=true | all-gather | bytes 9216 | tf_op jit(solution)/shard_map/all_gather | solution.py:97
  163.4 9.4 %all-gather.13.cloned.1.call-done = bf16[1024,2048]{1,0:T(8,128)(2,1)} async-done(((bf16[1024,512]{1,0:T(8,128)(2,1)}), bf16[1024,2048]{1,0:T(8,128)(2,1)}) %all-gather.13.cloned.1.call-update) | async-done | bytes 4194320 | tf_op jit(solution)/shard_map/all_gather | solution.py:55
  172.8 3.1 fusion.3
  175.9 97.7 %all-gather.15.cloned.1.call-done = bf16[2048,1536]{1,0:T(8,128)(2,1)} async-done(((bf16[256,1536]{1,0:T(8,128)(2,1)}), bf16[2048,1536]{1,0:T(8,128)(2,1)}) %all-gather.15.cloned.1.call-update) | async-done | bytes 6291472 | tf_op jit(solution)/shard_map/all_gather | solution.py:101
  273.6 11.7 %fusion.8 = f32[1024,1536]{1,0:T(8,128)} fusion(bf16[2048,1536]{1,0:T(8,128)(2,1)} %all-gather.15.cloned.1.call-done, bf16[1024,2048]{1,0:T(8,128)(2,1)} %all-gather.13.cloned.1.call-done, f32[2048]{0:T(1024)S(1)} %copy-done.6), kind=kOutput, calls=%fused_computation.13 | convolution fusion | flops 6448742400 | bytes 16785408 | tf_op jit(solution)/shard_map/dot_general | solution.py:59
  285.3 87.2 %all-gather.17.cloned.1.call-done = bf16[2048,1536]{1,0:T(8,128)(2,1)} async-done(((bf16[256,1536]{1,0:T(8,128)(2,1)}), bf16[2048,1536]{1,0:T(8,128)(2,1)}) %all-gather.17.cloned.1.call-update) | async-done | bytes 6291472 | tf_op jit(solution)/shard_map/all_gather | solution.py:102
  372.5 99.7 %all-gather.19.cloned.1.call-done = bf16[1536,2048]{1,0:T(8,128)(2,1)} async-done(((bf16[1536,256]{1,0:T(8,128)(2,1)}), bf16[1536,2048]{1,0:T(8,128)(2,1)}) %all-gather.19.cloned.1.call-update) | async-done | bytes 6291472 | tf_op jit(solution)/shard_map/all_gather | solution.py:70
  472.3 21.6 %multiply_convert_fusion = bf16[1024,2048]{1,0:T(8,128)(2,1)} fusion(bf16[1536,2048]{1,0:T(8,128)(2,1)} %all-gather.19.cloned.1.call-done, f32[2048]{0:T(1024)S(1)} %bitcast.59, f32[1024,1536]{1,0:T(8,128)} %fusion.8, bf16[2048,1536]{1,0:T(8,128)(2,1)} %all-gather.17.cloned.1.call-done, bf16[1024,2048]{1,0:T(8,128)(2,1)} %all-gather.13.cloned.1.call-done, ...), kind=kOutput, calls=%fused_computation.8 | convolution fusion | flops 12911116288 | bytes 27295744 | tf_op jit(solution)/shard_map/dot_general | solution.py:68
  493.9 42.8 %reduce-scatter.5.cloned.1.call-done = bf16[1024,512]{1,0:T(8,128)(2,1)} async-done(((bf16[1024,2048]{1,0:T(8,128)(2,1)}), bf16[1024,512]{1,0:T(8,128)(2,1)}) %reduce-scatter.5.cloned.1.call-update) | async-done | bytes 1048592 | tf_op jit(solution)/shard_map/reduce_scatter | solution.py:75
  536.7 2.5 add_convert_fusion
  (49 shorter events, 0.3 us)
Async XLA Ops:
  6.5 50.1 %copy-start.5 = (f32[2048]{0:T(1024)S(1)}, f32[2048]{0:T(1024)}, u32[]{:S(2)}) copy-start(f32[2048]{0:T(1024)} %param.14) | copy-start | bytes 24580
  6.5 50.1 %copy-start.9 = (f32[256]{0:T(256)S(1)}, f32[256]{0:T(256)}, u32[]{:S(2)}) copy-start(f32[256]{0:T(256)} %param.16) | copy-start | bytes 3076
  6.5 39.6 %all-gather.9.cloned.1.call-start = ((), (), s32[]{:S(2)}) async-start(), calls=%async_computation.2 | async-start | bytes 5242880 | tf_op jit(solution)/shard_map/all_gather | solution.py:55
  7.3 80.3 %all-gather.11.cloned.1.call-start = ((), (), s32[]{:S(2)}) async-start(), calls=%async_computation.3 | async-start | bytes 1179648 | tf_op jit(solution)/shard_map/all_gather | solution.py:70
  8.3 6.6 %collective-permute-start = (bf16[256,256]{1,0:T(8,128)(2,1)S(1)}, bf16[256,256]{1,0:T(8,128)(2,1)S(1)}, u32[]{:S(2)}, u32[]{:S(2)}) collective-permute-start(bf16[256,256]{1,0:T(8,128)(2,1)S(1)} %convert_element_type.145), channel_id=1, source_target_pairs={{0,4},{4,0},{8,12},{12,8},{16,20},{20,16},{24,28},{28,24},{1,5},{5... | collective-permute-start | bytes 393224 | tf_op jit(solution)/shard_map/ppermute | solution.py:18
  13.0 122.7 %reduce-scatter.3.cloned.1.call-start = ((), (), s32[]{:S(2)}) async-start(), calls=%async_computation.4 | async-start | bytes 5242880 | tf_op jit(solution)/shard_map/reduce_scatter | solution.py:75
  14.9 21.9 %collective-permute-start.1 = (bf16[512,256]{1,0:T(8,128)(2,1)S(1)}, bf16[512,256]{1,0:T(8,128)(2,1)S(1)}, u32[]{:S(2)}, u32[]{:S(2)}) collective-permute-start(bf16[512,256]{1,0:T(8,128)(2,1)S(1)} %maximum_select_fusion.3), channel_id=1, source_target_pairs={{0,8},{4,12},{8,0},{12,4},{16,24},{20,28},{24,16},{28,20},{1,9},{5... | collective-permute-start | bytes 786440 | tf_op jit(solution)/shard_map/ppermute | solution.py:18
  37.1 19.5 %collective-permute-start.2 = (bf16[1024,256]{1,0:T(8,128)(2,1)S(1)}, bf16[1024,256]{1,0:T(8,128)(2,1)S(1)}, u32[]{:S(2)}, u32[]{:S(2)}) collective-permute-start(bf16[1024,256]{1,0:T(8,128)(2,1)S(1)} %maximum_select_fusion.2), channel_id=1, source_target_pairs={{0,16},{4,20},{8,24},{12,28},{16,0},{20,4},{24,8},{28,12},{1,17},{... | collective-permute-start | bytes 1572872 | tf_op jit(solution)/shard_map/ppermute | solution.py:18
  87.6 48.1 %copy-start.1 = (bf16[1024,512]{1,0:T(8,128)(2,1)S(1)}, bf16[1024,512]{1,0:T(8,128)(2,1)}, u32[]{:S(2)}) copy-start(bf16[1024,512]{1,0:T(8,128)(2,1)} %param.13) | copy-start | bytes 3145732
  92.1 46.2 %copy-start.2 = (f32[256,1536]{1,0:T(8,128)S(1)}, f32[256,1536]{1,0:T(8,128)}, u32[]{:S(2)}) copy-start(f32[256,1536]{1,0:T(8,128)} %param.20) | copy-start | bytes 4718596
  92.1 50.8 %copy-start.4 = (f32[256]{0:T(256)S(1)}, f32[256]{0:T(256)}, u32[]{:S(2)}) copy-start(f32[256]{0:T(256)} %param.25) | copy-start | bytes 3076
  92.2 80.7 %all-gather.13.cloned.1.call-start = ((), (), s32[]{:S(2)}) async-start(), calls=%async_computation.5 | async-start | bytes 5242880 | tf_op jit(solution)/shard_map/all_gather | solution.py:55
  138.2 3.7 copy-start.3
  138.2 135.4 %copy-start.6 = (f32[2048]{0:T(1024)S(1)}, f32[2048]{0:T(1024)}, u32[]{:S(2)}) copy-start(f32[2048]{0:T(1024)} %param.19) | copy-start | bytes 24580
  138.2 135.4 %all-gather.15.cloned.1.call-start = ((), (), s32[]{:S(2)}) async-start(), calls=%async_computation.6 | async-start | bytes 7077888 | tf_op jit(solution)/shard_map/all_gather | solution.py:101
  139.3 233.2 %all-gather.17.cloned.1.call-start = ((), (), s32[]{:S(2)}) async-start(), calls=%async_computation.7 | async-start | bytes 7077888 | tf_op jit(solution)/shard_map/all_gather | solution.py:102
  141.8 330.5 %all-gather.19.cloned.1.call-start = ((), (), s32[]{:S(2)}) async-start(), calls=%async_computation.8 | async-start | bytes 7077888 | tf_op jit(solution)/shard_map/all_gather | solution.py:70
  142.9 393.8 %reduce-scatter.5.cloned.1.call-start = ((), (), s32[]{:S(2)}) async-start(), calls=%async_computation.9 | async-start | bytes 5242880 | tf_op jit(solution)/shard_map/reduce_scatter | solution.py:75
  175.9 296.4 %copy-start.7 = (f32[1536]{0:T(1024)S(1)}, f32[1536]{0:T(1024)}, u32[]{:S(2)}) copy-start(f32[1536]{0:T(1024)} %param.23) | copy-start | bytes 18436
  175.9 296.3 %copy-start.8 = (f32[1536]{0:T(1024)S(1)}, f32[1536]{0:T(1024)}, u32[]{:S(2)}) copy-start(f32[1536]{0:T(1024)} %param.21) | copy-start | bytes 18436
  472.3 64.4 %copy-start = (bf16[1024,512]{1,0:T(8,128)(2,1)S(1)}, bf16[1024,512]{1,0:T(8,128)(2,1)}, u32[]{:S(2)}) copy-start(bf16[1024,512]{1,0:T(8,128)(2,1)} %add_convert_fusion.1) | copy-start | bytes 3145732
Sparse Core Ops, SparseCore 0:
  8.9 37.1 all-gather.8
  48.1 39.3 all-gather.10
  92.3 43.4 reduce-scatter.2
  138.3 34.4 all-gather.12
  174.9 98.6 all-gather.14
  275.6 96.8 all-gather.16
  374.6 97.6 all-gather.18
  494.0 42.5 reduce-scatter.4
